TPU v7x, 32 devices: a whole 2x2x4 slice. The times are simulated.
32 devices in a mesh: sp: 8 (over z, y), tp: 4 (over x, core).
Axes of the slice: x: 2, y: 2, z: 4, core: 2. Of those that a mesh axis runs over, the one named last changes fastest.
Arguments:
- stream: bfloat16 [8192, 4096], P('sp', 'tp'), may hold values from -11 to 11
- norm_gain: bfloat16 [3, 4096], P(None, 'tp'), may hold values from 0.099609375 to 1.8984375
- pool_weight: bfloat16 [3, 4, 1024, 1024], P(None, 'tp', 'sp'), may hold values from -0.1875 to 0.1875
- pool_scale: bfloat16 [3, 4096], P(None, 'tp'), may hold values from 0.099609375 to 1.8984375
Outputs:
- mixed: bfloat16 [8192, 4096], P('sp', 'tp')
All inputs are finite; a program needn't handle non-finite values.
Results may differ from a plain program's by a relative error of at most 0.015.
Values may be sent and summed in bfloat16 or wider, within the bound.
A program may use at most 64 MiB of HBM per device.

v0:
```python
import jax
import jax.numpy as jnp
from jax import lax
from jax.sharding import PartitionSpec as P

D = 4096
POOL_GROUPS = 4
norm_eps = 1e-06


def padded(value, sides, width):
    for axis, dim in sides:
        devices, length = (lax.axis_size(axis), value.shape[dim])
        up = [(i, (i + 1) % devices) for i in range(devices - 1)]
        down = [(j, i) for i, j in up]
        last = lax.slice_in_dim(value, length - width, length, axis=dim)
        initial = lax.slice_in_dim(value, 0, width, axis=dim)
        before = lax.ppermute(last, axis, up)
        after = lax.ppermute(initial, axis, down)
        value = jnp.concatenate([before, value, after], axis=dim)
    return value


def window_pool(extended, out_rows, centre, halves, seq_total, reach_rows, per_dev, group_width):
    ext_float = extended.astype(jnp.float32).reshape(extended.shape[0], per_dev, group_width)
    window_sums = jnp.zeros((out_rows, per_dev, group_width), jnp.float32)
    for offset in range(-reach_rows, reach_rows):
        in_window = ((offset >= -halves) & (offset < halves)).astype(jnp.float32)
        window_sums = (
            window_sums
            + ext_float[reach_rows + offset : reach_rows + offset + out_rows]
            * in_window[None, :, None]
        )
    low_end = jnp.maximum(centre[:, None] - halves[None, :], 0)
    high_end = jnp.minimum(centre[:, None] + halves[None, :], seq_total)
    counts = jnp.maximum(high_end - low_end, 1).astype(jnp.float32)
    middle = ext_float[reach_rows : reach_rows + out_rows]
    return (window_sums / counts[:, :, None] - middle).astype(jnp.bfloat16)


def local(stream, norm_gain, pool_weight, pool_scale):
    tok_rows, local_width = stream.shape
    layers, per_dev, shard_rows, group_width = pool_weight.shape
    reach_rows = 2**POOL_GROUPS // 2
    seq_total = tok_rows * lax.axis_size("sp")
    first_pos = lax.axis_index("sp") * tok_rows
    groups = lax.axis_index("tp") * per_dev + jnp.arange(per_dev, dtype=jnp.int32)
    halves = jnp.left_shift(jnp.int32(1), groups)
    deep_rows = reach_rows * layers
    current = padded(stream, (("sp", 0),), deep_rows)
    base_pos = first_pos - deep_rows
    for layer_idx in range(layers):
        ext_rows = current.shape[0]
        positions = base_pos + jnp.arange(ext_rows, dtype=jnp.int32)
        inside = (positions >= 0) & (positions < seq_total)
        current_f = current.astype(jnp.float32)
        square_sums = lax.psum(jnp.sum(current_f * current_f, axis=1), "tp")
        row_scale = lax.rsqrt(square_sums / D + norm_eps)
        normed = current_f * row_scale[:, None] * norm_gain[layer_idx].astype(jnp.float32)
        normed = jnp.where(inside[:, None], normed, 0.0).astype(jnp.bfloat16)
        out_rows = ext_rows - 2 * reach_rows
        residual = current_f[reach_rows : ext_rows - reach_rows]
        centre = positions[reach_rows : ext_rows - reach_rows]
        base_pos = base_pos + reach_rows
        pooled = window_pool(
            normed, out_rows, centre, halves, seq_total, reach_rows, per_dev, group_width
        )
        branch = jnp.einsum(
            "tgc,gcd->tgd",
            pooled,
            lax.all_gather(pool_weight[layer_idx], "sp", axis=1, tiled=True),
            preferred_element_type=jnp.float32,
        )
        branch = branch.reshape(out_rows, local_width)
        current = (residual + branch * pool_scale[layer_idx].astype(jnp.float32)).astype(
            jnp.bfloat16
        )
    return current


def solution(mesh):
    placed = (P("sp", "tp"), P(None, "tp"), P(None, "tp", "sp", None), P(None, "tp"))
    return jax.shard_map(
        local, mesh=mesh, in_specs=placed, out_specs=P("sp", "tp"), check_vma=False
    )
```

profile of v0, /device:TPU:0, one launch (start us, length us, event | category | flops | bytes accessed | tf_op | source)
XLA Modules:
  0.0 213.5 jit_solution(14513719529926578591)
XLA Ops:
  6.5 0.0 copy-start
  6.5 0.0 all-gather.7.cloned.1.call-start
  6.5 2.2 %fusion.70 = (bf16[1,1,128,1024]{3,2,1,0:T(8,128)(2,1)}, bf16[1,1,128,1024]{3,2,1,0:T(8,128)(2,1)}, bf16[1,1,128,1024]{3,2,1,0:T(8,128)(2,1)}) fusion(bf16[3,1,128,1024]{3,2,1,0:T(8,128)(2,1)} %param.6), kind=kLoop, calls=%fused_computation.141 | loop fusion | bytes 1572864 | tf_op jit(solution)/shard_map/slice | solution.py:71
  8.7 0.0 all-gather.7.cloned.1.call-update
  8.7 0.0 all-gather.9.cloned.1.call-start
  8.8 0.7 all-gather.9.cloned.1.call-update
  9.5 0.0 all-gather.11.cloned.1.call-start
  9.5 0.8 fusion.69
  10.4 4.9 %collective-permute-start = (bf16[24,1024]{1,0:T(8,128)(2,1)S(1)}, bf16[24,1024]{1,0:T(8,128)(2,1)S(1)}, u32[]{:S(2)}, u32[]{:S(2)}) collective-permute-start(bf16[24,1024]{1,0:T(8,128)(2,1)S(1)} %get-tuple-element.5), channel_id=1, source_target_pairs={{0,4},{4,8},{8,12},{12,16},{16,20},{20,24},{24,28},{1,5},{5,9},{9,... | collective-permute-start | bytes 147464 | tf_op jit(solution)/shard_map/ppermute | solution.py:18
  15.3 1.3 collective-permute-start.1
  16.6 0.0 all-gather.11.cloned.1.call-update
  16.6 0.8 slice_convert_fusion.1
  17.5 0.8 slice_convert_fusion
  18.3 0.1 maximum_convert_fusion.2
  18.4 0.1 maximum_convert_fusion.1
  18.5 0.1 maximum_convert_fusion.3
  18.7 0.0 collective-permute-done
  18.7 2.5 %collective-permute-done.1 = bf16[24,1024]{1,0:T(8,128)(2,1)S(1)} collective-permute-done((bf16[24,1024]{1,0:T(8,128)(2,1)S(1)}, bf16[24,1024]{1,0:T(8,128)(2,1)S(1)}, u32[]{:S(2)}, u32[]{:S(2)}) %collective-permute-start.1) | collective-permute-done | bytes 49184 | tf_op jit(solution)/shard_map/ppermute | solution.py:19
  21.2 0.0 copy-done
  21.2 0.5 multiply_reduce_fusion
  21.8 6.2 %psum.21 = f32[1072]{0:T(1024)S(1)} all-reduce(f32[1072]{0:T(1024)S(1)} %multiply_reduce_fusion), channel_id=1, replica_groups=mesh['sp'=8,'tp'=4] {'tp'}, use_global_device_ids=true, to_apply=%region_1.0 | all-reduce | flops 1072 | bytes 8576 | tf_op jit(solution)/shard_map/psum | solution.py:57
  27.9 2.5 %maximum_convert_fusion = f32[1072,1024]{1,0:T(8,128)} fusion(bf16[24,1024]{1,0:T(8,128)(2,1)S(1)} %collective-permute-done.1, bf16[1024,1024]{1,0:T(8,128)(2,1)S(1)} %copy-done, bf16[24,1024]{1,0:T(8,128)(2,1)S(1)} %collective-permute-done), kind=kLoop, calls=%fused_computation.115 | loop fusion | flops 6586368 | bytes 6586368 | tf_op jit(solution)/shard_map/convert_element_type | solution.py:56
  30.5 2.9 %fusion.59 = f32[1072,1024]{1,0:T(8,128)} fusion(f32[1024]{0:T(1024)S(1)} %bitcast.21, f32[1072]{0:T(1024)S(1)} %add_rsqrt_fusion.2, pred[1072]{0:T(1024)(128)(4,1)S(1)} %compare_and_fusion.2, bf16[24,1024]{1,0:T(8,128)(2,1)S(1)} %collective-permute-done.1, bf16[1024,1024]{1,0:T(8,128)(2,1)S(1)} %copy-done, bf16[24,1024]{1,0:T(8,128)(2,1)S(1)} %collective-permute-done), kind=kLoop, calls=%fused_computation.114 | loop fusion | flops 12075008 | bytes 6595824 | tf_op jit(solution)/shard_map/convert_element_type | solution.py:25
  33.4 28.0 %all-gather.7.cloned.1.call-done = bf16[1,1,1024,1024]{3,2,1,0:T(8,128)(2,1)} async-done(((bf16[1,1,128,1024]{3,2,1,0:T(8,128)(2,1)}), bf16[1,1,1024,1024]{3,2,1,0:T(8,128)(2,1)}) %all-gather.7.cloned.1.call-update) | async-done | bytes 2097168 | tf_op jit(solution)/shard_map/all_gather | solution.py:71
  61.4 42.3 %multiply_reduce_fusion.1 = (f32[1056]{0:T(1024)S(1)}, f32[1056,1024]{1,0:T(8,128)}) fusion(f32[1024]{0:T(1024)S(1)} %bitcast.24, bf16[1,1,1024,1024]{3,2,1,0:T(8,128)(2,1)} %all-gather.7.cloned.1.call-done, f32[1072,1024]{1,0:T(8,128)} %fusion.59, f32[1056]{0:T(1024)S(1)} %maximum_convert_fusion.2, f32[]{:T(128)S(6)} %mul.631, f32[]{:T(128)S(6)} %mul.628, ...), kind=kOutput, calls=%fused_computation.40 | convolution fusion | flops 2257845248 | bytes 79966528 | tf_op jit(solution)/shard_map/tgc,gcd->tgd/dot_general | solution.py:68
  103.7 6.3 %psum.22 = f32[1056]{0:T(1024)S(1)} all-reduce(f32[1056]{0:T(1024)S(1)} %get-tuple-element.16), channel_id=1, replica_groups=mesh['sp'=8,'tp'=4] {'tp'}, use_global_device_ids=true, to_apply=%region_3.4 | all-reduce | flops 1056 | bytes 8448 | tf_op jit(solution)/shard_map/psum | solution.py:57
  110.0 4.7 %fusion.60 = f32[1056,1024]{1,0:T(8,128)} fusion(f32[1056,1024]{1,0:T(8,128)} %get-tuple-element.17, f32[1024]{0:T(1024)S(1)} %bitcast.20, f32[1056]{0:T(1024)S(1)} %add_rsqrt_fusion.1, pred[1056]{0:T(1024)(128)(4,1)S(1)} %compare_and_fusion.1), kind=kLoop, calls=%fused_computation.116 | loop fusion | flops 5406720 | bytes 8660128 | tf_op jit(solution)/shard_map/convert_element_type | solution.py:25
  114.8 0.0 all-gather.9.cloned.1.call-done
  114.8 41.7 %multiply_reduce_fusion.2 = (f32[1040]{0:T(1024)S(1)}, f32[1040,1024]{1,0:T(8,128)}) fusion(f32[1024]{0:T(1024)S(1)} %bitcast.23, bf16[1,1,1024,1024]{3,2,1,0:T(8,128)(2,1)} %all-gather.9.cloned.1.call-done, f32[1056,1024]{1,0:T(8,128)} %fusion.60, f32[1040]{0:T(1024)S(1)} %maximum_convert_fusion.1, f32[]{:T(128)S(6)} %mul.631, f32[]{:T(128)S(6)} %mul.628, ...), kind=kOutput, calls=%fused_computation.75 | convolution fusion | flops 2223635456 | bytes 78786752 | tf_op jit(solution)/shard_map/tgc,gcd->tgd/dot_general | solution.py:68
  156.4 6.7 %psum.23 = f32[1040]{0:T(1024)S(1)} all-reduce(f32[1040]{0:T(1024)S(1)} %get-tuple-element.18), channel_id=1, replica_groups=mesh['sp'=8,'tp'=4] {'tp'}, use_global_device_ids=true, to_apply=%region_5.6 | all-reduce | flops 1040 | bytes 8320 | tf_op jit(solution)/shard_map/psum | solution.py:57
  163.1 4.7 %fusion.63 = f32[1040,1024]{1,0:T(8,128)} fusion(f32[1040,1024]{1,0:T(8,128)} %get-tuple-element.19, f32[1024]{0:T(1024)S(1)} %bitcast.19, f32[1040]{0:T(1024)S(1)} %add_rsqrt_fusion, pred[1040]{0:T(1024)(128)(4,1)S(1)} %compare_and_fusion), kind=kLoop, calls=%fused_computation.118 | loop fusion | flops 5324800 | bytes 8528976 | tf_op jit(solution)/shard_map/convert_element_type | solution.py:25
  167.8 0.0 all-gather.11.cloned.1.call-done
  167.8 39.2 %fusion.55 = bf16[1024,1024]{1,0:T(8,128)(2,1)} fusion(f32[1040,1024]{1,0:T(8,128)} %get-tuple-element.19, bf16[1,1,1024,1024]{3,2,1,0:T(8,128)(2,1)} %all-gather.11.cloned.1.call-done, f32[1024]{0:T(1024)S(1)} %bitcast.22, f32[1040,1024]{1,0:T(8,128)} %fusion.63, f32[1024]{0:T(1024)S(1)} %maximum_convert_fusion.3, f32[]{:T(128)S(6)} %mul.631, ...), kind=kOutput, calls=%fused_computation.110 | convolution fusion | flops 2186280960 | bytes 75505728 | tf_op jit(solution)/shard_map/tgc,gcd->tgd/dot_general | solution.py:68
  (9 shorter events, 0.1 us)
Async XLA Ops:
  6.5 14.7 %copy-start = (bf16[1024,1024]{1,0:T(8,128)(2,1)S(1)}, bf16[1024,1024]{1,0:T(8,128)(2,1)}, u32[]{:S(2)}) copy-start(bf16[1024,1024]{1,0:T(8,128)(2,1)} %param.4) | copy-start | bytes 6291460
  6.5 54.9 %all-gather.7.cloned.1.call-start = ((), (), s32[]{:S(2)}) async-start(), calls=%async_computation | async-start | bytes 2359296 | tf_op jit(solution)/shard_map/all_gather | solution.py:71
  8.7 106.1 %all-gather.9.cloned.1.call-start = ((), (), s32[]{:S(2)}) async-start(), calls=%async_computation.1 | async-start | bytes 2359296 | tf_op jit(solution)/shard_map/all_gather | solution.py:71
  9.5 158.3 %all-gather.11.cloned.1.call-start = ((), (), s32[]{:S(2)}) async-start(), calls=%async_computation.2 | async-start | bytes 2359296 | tf_op jit(solution)/shard_map/all_gather | solution.py:71
  10.4 8.3 %collective-permute-start = (bf16[24,1024]{1,0:T(8,128)(2,1)S(1)}, bf16[24,1024]{1,0:T(8,128)(2,1)S(1)}, u32[]{:S(2)}, u32[]{:S(2)}) collective-permute-start(bf16[24,1024]{1,0:T(8,128)(2,1)S(1)} %get-tuple-element.5), channel_id=1, source_target_pairs={{0,4},{4,8},{8,12},{12,16},{16,20},{20,24},{24,28},{1,5},{5,9},{9,... | collective-permute-start | bytes 147464 | tf_op jit(solution)/shard_map/ppermute | solution.py:18
  15.3 6.0 %collective-permute-start.1 = (bf16[24,1024]{1,0:T(8,128)(2,1)S(1)}, bf16[24,1024]{1,0:T(8,128)(2,1)S(1)}, u32[]{:S(2)}, u32[]{:S(2)}) collective-permute-start(bf16[24,1024]{1,0:T(8,128)(2,1)S(1)} %get-tuple-element.6), channel_id=1, source_target_pairs={{4,0},{8,4},{12,8},{16,12},{20,16},{24,20},{28,24},{5,1},{9,5},{13... | collective-permute-start | bytes 147464 | tf_op jit(solution)/shard_map/ppermute | solution.py:19
Sparse Core Ops, SparseCore 0:
  9.5 51.8 all-gather.6
  63.5 47.6 all-gather.8
  113.3 47.6 all-gather.10
where the time goes:
time: 214 us
  matrix products  123 us (57%)
  waiting for transfers between devices  31.3 us (15%)
  blocking collectives  19.2 us (9%)
  other arithmetic  17.3 us (8%)
  between operations  13.4 us (6%)
  starting transfers between devices  6.26 us (3%)
  local copies, waits for them, and re-layouts  3 us (1%)
    dot_general x3, matrix products, local(): jnp.einsum('tgc,gcd->tgd', pooled, lax.all_gather(pool_weight[layer_idx],...  123 us
    all_gather x3, waiting for transfers between devices, local(): lax.all_gather(pool_weight[layer_idx], 'sp', axis=1, tiled=True)  28 us
    psum x3, blocking collectives, local(): square_sums = lax.psum(jnp.sum(current_f * current_f, axis=1), 'tp')  19.2 us
    convert_element_type x3, other arithmetic, window_pool(): extended.astype(jnp.float32)  12.3 us
    ppermute x1, starting transfers between devices, padded(): before = lax.ppermute(last, axis, up)  4.89 us
  transfers between devices with their start and end apart: 5, of which 2 were waited for; matrix products, arithmetic and copies ran while one was open for 48% of the time, Pallas kernels for 0%

commit v1 on v0

--- a/solution.py
+++ b/solution.py
@@ -54,7 +54,7 @@
         positions = base_pos + jnp.arange(ext_rows, dtype=jnp.int32)
         inside = (positions >= 0) & (positions < seq_total)
         current_f = current.astype(jnp.float32)
-        square_sums = lax.psum(jnp.sum(current_f * current_f, axis=1), "tp")
+        square_sums = jnp.sum(lax.all_gather(jnp.sum(current_f * current_f, axis=1), "tp"), axis=0)
         row_scale = lax.rsqrt(square_sums / D + norm_eps)
         normed = current_f * row_scale[:, None] * norm_gain[layer_idx].astype(jnp.float32)
         normed = jnp.where(inside[:, None], normed, 0.0).astype(jnp.bfloat16)

time: 214 us -> 223 us (1.042)
  blocking collectives: 19.2 us -> 32 us
  waiting for transfers between devices: 31.3 us -> 22.8 us
  local copies, waits for them, and re-layouts: 3 us -> 5.54 us
    unnamed x0 -> x3, blocking collectives: none -> 32 us
    psum x3 -> x0, blocking collectives: 19.2 us -> none  [local(): square_sums = lax.psum(jnp.sum(current_f * current_f, axis=1), 'tp')]
    all_gather x3, waiting for transfers between devices: 28 us -> 22 us  [local(): lax.all_gather(pool_weight[layer_idx], 'sp', axis=1, tiled=True)]
    ppermute x1, waiting for transfers between devices: 2.54 us -> 0.01 us  [padded(): after = lax.ppermute(initial, axis, down)]
    unnamed x2 -> x9, local copies, waits for them, and re-layouts: 0.01 us -> 2.3 us
  transfers between devices with their start and end apart: 5 -> 5, of which waited for: 2 -> 1; matrix products, arithmetic and copies ran while one was open for 48% -> 47% of each run, Pallas kernels for 0% -> 0%
where the time goes in v1:
time: 223 us; the launch traced here: 222 us
  matrix products  123 us (55%)
  blocking collectives  32 us (14%)
  waiting for transfers between devices  22.8 us (10%)
  other arithmetic  17.4 us (8%)
  between operations  15.4 us (7%)
  starting transfers between devices  6.26 us (3%)
  local copies, waits for them, and re-layouts  5.54 us (2%)
    dot_general x3, matrix products, local(): jnp.einsum('tgc,gcd->tgd', pooled, lax.all_gather(pool_weight[layer_idx],...  123 us
    unnamed x3, blocking collectives  32 us
    all_gather x3, waiting for transfers between devices, local(): lax.all_gather(pool_weight[layer_idx], 'sp', axis=1, tiled=True)  22 us
    convert_element_type x3, other arithmetic, window_pool(): extended.astype(jnp.float32)  12.3 us
    ppermute x1, starting transfers between devices, padded(): before = lax.ppermute(last, axis, up)  4.89 us
  transfers between devices with their start and end apart: 5, of which 1 were waited for; matrix products, arithmetic and copies ran while one was open for 47% of the time, Pallas kernels for 0%

profile of v1, /device:TPU:0, one launch (start us, length us, event | category | flops | bytes accessed | tf_op | source)
XLA Modules:
  0.0 222.4 jit_solution(346212120320951949)
XLA Ops:
  6.5 0.0 copy-start
  6.5 0.0 all-gather.10.cloned.1.call-start
  6.5 2.2 fusion.70
  8.7 0.0 all-gather.10.cloned.1.call-update
  8.7 0.0 all-gather.12.cloned.1.call-start
  8.8 0.7 all-gather.12.cloned.1.call-update
  9.5 0.0 all-gather.14.cloned.1.call-start
  9.5 0.8 fusion.69
  10.4 4.9 %collective-permute-start = (bf16[24,1024]{1,0:T(8,128)(2,1)S(1)}, bf16[24,1024]{1,0:T(8,128)(2,1)S(1)}, u32[]{:S(2)}, u32[]{:S(2)}) collective-permute-start(bf16[24,1024]{1,0:T(8,128)(2,1)S(1)} %get-tuple-element.5), channel_id=1, source_target_pairs={{0,4},{4,8},{8,12},{12,16},{16,20},{20,24},{24,28},{1,5},{5,9},{9,... | collective-permute-start | bytes 147464 | tf_op jit(solution)/shard_map/ppermute | solution.py:18
  15.3 1.3 collective-permute-start.1
  16.6 0.0 all-gather.14.cloned.1.call-update
  16.6 0.8 slice_convert_fusion.1
  17.5 0.8 slice_convert_fusion
  18.3 0.1 maximum_convert_fusion.2
  18.4 0.1 maximum_convert_fusion.1
  18.5 0.1 maximum_convert_fusion.3
  18.7 1.3 dynamic-slice
  22.0 0.0 collective-permute-done
  22.0 0.0 collective-permute-done.1
  22.0 0.0 copy-done
  22.0 0.5 multiply_reduce_fusion
  22.6 0.3 dynamic-update-slice
  22.9 10.9 %all-reduce = f32[4288]{0:T(1024)S(1)} all-reduce(f32[4288]{0:T(1024)S(1)} %dynamic-update-slice), channel_id=2, replica_groups=mesh['sp'=8,'tp'=4] {'tp'}, use_global_device_ids=true, to_apply=%add | all-reduce | flops 4288 | bytes 34304
  33.8 0.1 reshape.457
  33.9 2.6 %maximum_convert_fusion = f32[1072,1024]{1,0:T(8,128)} fusion(bf16[24,1024]{1,0:T(8,128)(2,1)S(1)} %collective-permute-done.1, bf16[1024,1024]{1,0:T(8,128)(2,1)S(1)} %copy-done, bf16[24,1024]{1,0:T(8,128)(2,1)S(1)} %collective-permute-done), kind=kLoop, calls=%fused_computation.115 | loop fusion | flops 6586368 | bytes 6586368 | tf_op jit(solution)/shard_map/convert_element_type | solution.py:56
  36.5 2.9 %fusion.59 = f32[1072,1024]{1,0:T(8,128)} fusion(f32[1024]{0:T(1024)S(1)} %bitcast.24, f32[1072]{0:T(1024)S(1)} %add_rsqrt_fusion.2, pred[1072]{0:T(1024)(128)(4,1)S(1)} %compare_and_fusion.2, bf16[24,1024]{1,0:T(8,128)(2,1)S(1)} %collective-permute-done.1, bf16[1024,1024]{1,0:T(8,128)(2,1)S(1)} %copy-done, bf16[24,1024]{1,0:T(8,128)(2,1)S(1)} %collective-permute-done), kind=kLoop, calls=%fused_computation.114 | loop fusion | flops 12075008 | bytes 6595824 | tf_op jit(solution)/shard_map/convert_element_type | solution.py:25
  39.4 22.0 %all-gather.10.cloned.1.call-done = bf16[1,1,1024,1024]{3,2,1,0:T(8,128)(2,1)} async-done(((bf16[1,1,128,1024]{3,2,1,0:T(8,128)(2,1)}), bf16[1,1,1024,1024]{3,2,1,0:T(8,128)(2,1)}) %all-gather.10.cloned.1.call-update) | async-done | bytes 2097168 | tf_op jit(solution)/shard_map/all_gather | solution.py:71
  61.4 42.1 %multiply_reduce_fusion.1 = (f32[1056]{0:T(1024)S(1)}, f32[1056,1024]{1,0:T(8,128)}) fusion(f32[1024]{0:T(1024)S(1)} %bitcast.27, bf16[1,1,1024,1024]{3,2,1,0:T(8,128)(2,1)} %all-gather.10.cloned.1.call-done, f32[1072,1024]{1,0:T(8,128)} %fusion.59, f32[1056]{0:T(1024)S(1)} %maximum_convert_fusion.2, f32[]{:T(128)S(6)} %mul.631, f32[]{:T(128)S(6)} %mul.628, ...), kind=kOutput, calls=%fused_computation.40 | convolution fusion | flops 2257845248 | bytes 79966528 | tf_op jit(solution)/shard_map/tgc,gcd->tgd/dot_general | solution.py:68
  103.5 0.3 dynamic-update-slice.1
  103.9 10.8 %all-reduce.1 = f32[4224]{0:T(1024)S(1)} all-reduce(f32[4224]{0:T(1024)S(1)} %dynamic-update-slice.1), channel_id=4, replica_groups=mesh['sp'=8,'tp'=4] {'tp'}, use_global_device_ids=true, to_apply=%add.1 | all-reduce | flops 4224 | bytes 33792
  114.7 0.1 reshape.459
  114.8 4.7 %fusion.60 = f32[1056,1024]{1,0:T(8,128)} fusion(f32[1056,1024]{1,0:T(8,128)} %get-tuple-element.17, f32[1024]{0:T(1024)S(1)} %bitcast.23, f32[1056]{0:T(1024)S(1)} %add_rsqrt_fusion.1, pred[1056]{0:T(1024)(128)(4,1)S(1)} %compare_and_fusion.1), kind=kLoop, calls=%fused_computation.116 | loop fusion | flops 5406720 | bytes 8660128 | tf_op jit(solution)/shard_map/convert_element_type | solution.py:25
  119.6 0.0 all-gather.12.cloned.1.call-done
  119.6 41.5 %multiply_reduce_fusion.2 = (f32[1040]{0:T(1024)S(1)}, f32[1040,1024]{1,0:T(8,128)}) fusion(f32[1024]{0:T(1024)S(1)} %bitcast.26, bf16[1,1,1024,1024]{3,2,1,0:T(8,128)(2,1)} %all-gather.12.cloned.1.call-done, f32[1056,1024]{1,0:T(8,128)} %fusion.60, f32[1040]{0:T(1024)S(1)} %maximum_convert_fusion.1, f32[]{:T(128)S(6)} %mul.631, f32[]{:T(128)S(6)} %mul.628, ...), kind=kOutput, calls=%fused_computation.75 | convolution fusion | flops 2223635456 | bytes 78786752 | tf_op jit(solution)/shard_map/tgc,gcd->tgd/dot_general | solution.py:68
  161.1 0.3 dynamic-update-slice.2
  161.4 10.3 %all-reduce.2 = f32[4160]{0:T(1024)S(1)} all-reduce(f32[4160]{0:T(1024)S(1)} %dynamic-update-slice.2), channel_id=6, replica_groups=mesh['sp'=8,'tp'=4] {'tp'}, use_global_device_ids=true, to_apply=%add.2 | all-reduce | flops 4160 | bytes 33280
  171.7 0.1 reshape.461
  171.8 4.7 %fusion.63 = f32[1040,1024]{1,0:T(8,128)} fusion(f32[1040,1024]{1,0:T(8,128)} %get-tuple-element.19, f32[1024]{0:T(1024)S(1)} %bitcast.22, f32[1040]{0:T(1024)S(1)} %add_rsqrt_fusion, pred[1040]{0:T(1024)(128)(4,1)S(1)} %compare_and_fusion), kind=kLoop, calls=%fused_computation.118 | loop fusion | flops 5324800 | bytes 8528976 | tf_op jit(solution)/shard_map/convert_element_type | solution.py:25
  176.5 0.0 all-gather.14.cloned.1.call-done
  176.5 39.4 %fusion.55 = bf16[1024,1024]{1,0:T(8,128)(2,1)} fusion(f32[1040,1024]{1,0:T(8,128)} %get-tuple-element.19, bf16[1,1,1024,1024]{3,2,1,0:T(8,128)(2,1)} %all-gather.14.cloned.1.call-done, f32[1024]{0:T(1024)S(1)} %bitcast.25, f32[1040,1024]{1,0:T(8,128)} %fusion.63, f32[1024]{0:T(1024)S(1)} %maximum_convert_fusion.3, f32[]{:T(128)S(6)} %mul.631, ...), kind=kOutput, calls=%fused_computation.110 | convolution fusion | flops 2186280960 | bytes 75505728 | tf_op jit(solution)/shard_map/tgc,gcd->tgd/dot_general | solution.py:68
  (15 shorter events, 0.1 us)
Async XLA Ops:
  6.5 15.5 %copy-start = (bf16[1024,1024]{1,0:T(8,128)(2,1)S(1)}, bf16[1024,1024]{1,0:T(8,128)(2,1)}, u32[]{:S(2)}) copy-start(bf16[1024,1024]{1,0:T(8,128)(2,1)} %param.4) | copy-start | bytes 6291460
  6.5 54.9 %all-gather.10.cloned.1.call-start = ((), (), s32[]{:S(2)}) async-start(), calls=%async_computation | async-start | bytes 2359296 | tf_op jit(solution)/shard_map/all_gather | solution.py:71
  8.7 110.8 %all-gather.12.cloned.1.call-start = ((), (), s32[]{:S(2)}) async-start(), calls=%async_computation.1 | async-start | bytes 2359296 | tf_op jit(solution)/shard_map/all_gather | solution.py:71
  9.5 167.0 %all-gather.14.cloned.1.call-start = ((), (), s32[]{:S(2)}) async-start(), calls=%async_computation.2 | async-start | bytes 2359296 | tf_op jit(solution)/shard_map/all_gather | solution.py:71
  10.4 11.7 %collective-permute-start = (bf16[24,1024]{1,0:T(8,128)(2,1)S(1)}, bf16[24,1024]{1,0:T(8,128)(2,1)S(1)}, u32[]{:S(2)}, u32[]{:S(2)}) collective-permute-start(bf16[24,1024]{1,0:T(8,128)(2,1)S(1)} %get-tuple-element.5), channel_id=1, source_target_pairs={{0,4},{4,8},{8,12},{12,16},{16,20},{20,24},{24,28},{1,5},{5,9},{9,... | collective-permute-start | bytes 147464 | tf_op jit(solution)/shard_map/ppermute | solution.py:18
  15.3 6.8 %collective-permute-start.1 = (bf16[24,1024]{1,0:T(8,128)(2,1)S(1)}, bf16[24,1024]{1,0:T(8,128)(2,1)S(1)}, u32[]{:S(2)}, u32[]{:S(2)}) collective-permute-start(bf16[24,1024]{1,0:T(8,128)(2,1)S(1)} %get-tuple-element.6), channel_id=1, source_target_pairs={{4,0},{8,4},{12,8},{16,12},{20,16},{24,20},{28,24},{5,1},{9,5},{13... | collective-permute-start | bytes 147464 | tf_op jit(solution)/shard_map/ppermute | solution.py:19
Sparse Core Ops, SparseCore 0:
  9.5 51.8 all-gather.9
  63.5 47.5 all-gather.11
  113.3 47.6 all-gather.13
